TPU v7x, 256 devices: a 8x8x2 block of a 8x8x16 slice. The times are simulated.
256 devices in a mesh: grp: 2 (over z), kv: 16 (over y, core), tp: 8 (over x).
Axes of the slice: x: 8, y: 8, z: 2, core: 2. Of those that a mesh axis runs over, the one named last changes fastest.
The devices are a block of a 8x8x16 slice.
Arguments:
- tokens: bfloat16 [256, 4096], P('grp', ('kv', 'tp')), parts along dimension 0, may hold values from -12 to 12
- gain_in: bfloat16 [4096], P(('kv', 'tp')), may hold values from 0.099609375 to 1.8984375
- gate_in: bfloat16 [4096, 11008], P('kv', 'tp'), may hold values from -0.09375 to 0.09375
- up_in: bfloat16 [4096, 11008], P('kv', 'tp'), may hold values from -0.09375 to 0.09375
- down_in: bfloat16 [11008, 4096], P('tp', 'kv'), may hold values from -0.21875 to 0.21875
- gain_mix: bfloat16 [4096], P(('kv', 'tp')), may hold values from 0.099609375 to 1.8984375
- w_query: bfloat16 [4096, 1024], P('kv', 'tp'), may hold values from -0.09375 to 0.09375
- w_key: bfloat16 [4096, 1024], P('kv', 'tp'), may hold values from -0.09375 to 0.09375
- w_value: bfloat16 [4096, 2048], P('kv', 'tp'), may hold values from -0.09375 to 0.09375
- w_gate: bfloat16 [4096, 2048], P('kv', 'tp'), may hold values from -0.09375 to 0.09375
- w_mixout: bfloat16 [2048, 4096], P('tp', 'kv'), may hold values from -0.125 to 0.125
- forget_rate: float32 [8], P('tp'), may hold values from 0.01 to 0.7
- state_in: float32 [256, 8, 128, 256], P(('grp', 'kv'), 'tp'), parts along dimension 0, may hold values from -0.6 to 0.6
- positions: int32 [256], P(('grp', 'kv')), parts along dimension 0, may hold values from 0 to 8191
- gain_out: bfloat16 [4096], P(('kv', 'tp')), may hold values from 0.099609375 to 1.8984375
- gate_out: bfloat16 [4096, 11008], P('kv', 'tp'), may hold values from -0.09375 to 0.09375
- up_out: bfloat16 [4096, 11008], P('kv', 'tp'), may hold values from -0.09375 to 0.09375
- down_out: bfloat16 [11008, 4096], P('tp', 'kv'), may hold values from -0.21875 to 0.21875
Outputs:
- result: bfloat16 [256, 4096], P('grp', ('kv', 'tp')), parts along dimension 0
- new_state: float32 [256, 8, 128, 256], P(('grp', 'kv'), 'tp'), parts along dimension 0
There are 2 independent parts, one for each index of `grp`. A program takes and returns all parts, laid end to end along the dimension named above; an argument that names none is the same for every part. Nothing has to cross between parts.
All inputs are finite; a program needn't handle non-finite values.
Results may differ from a plain program's by a relative error of at most 0.024.
Values may be sent and summed in bfloat16 or wider, within the bound.
A program may use at most 64 MiB of HBM per device.

v0:
```python
import jax
import jax.numpy as jnp
from jax import lax
from jax.sharding import Mesh
from jax.sharding import PartitionSpec as P

D = 4096
DK = 128
DV = 256
KV_TP = ("kv_0", "kv_1", "tp")
KV = ("kv_0", "kv_1")
GRP_KV = ("grp", "kv_0", "kv_1")


epsilon = 1e-06


def by_axis(value, axes):
    for axis in axes:
        value = lax.psum(value, axis)
    return value


def in_order(tiles, dim):
    lengths = list(tiles.shape[1:])
    lengths[dim] *= tiles.shape[0]
    return jnp.moveaxis(tiles, 0, dim).reshape(lengths)


def sent_to_all(value, axis):
    count = lax.axis_size(axis)
    return lax.all_to_all(
        jnp.broadcast_to(value[None], (count, *value.shape)), axis, 0, 0, tiled=True
    )


def collect(value, axis, dim):
    return in_order(sent_to_all(value, axis), dim)


def cut_along(value, dim, count):
    before, after = (value.shape[:dim], value.shape[dim + 1 :])
    return jnp.moveaxis(value.reshape(*before, count, -1, *after), dim, 0)


def sum_at_owner(value, axis, dim):
    tiles = cut_along(value, dim, lax.axis_size(axis))
    arrived = lax.all_to_all(tiles, axis, split_axis=0, concat_axis=0, tiled=True)
    return arrived.astype(jnp.float32).sum(axis=0)


def rotate(vectors, positions):
    half_dim = vectors.shape[-1] // 2
    inverse = jnp.power(10000.0, -jnp.arange(half_dim, dtype=jnp.float32) * 2.0 / vectors.shape[-1])
    angles = positions.astype(jnp.float32)[:, None] * inverse[None, :]
    cosine = jnp.cos(angles)[:, None, :]
    sine_part = jnp.sin(angles)[:, None, :]
    first_half = vectors[..., :half_dim]
    second_half = vectors[..., half_dim:]
    return jnp.concatenate(
        [
            first_half * cosine - second_half * sine_part,
            first_half * sine_part + second_half * cosine,
        ],
        axis=-1,
    )


def block_rows(tokens, gain_row):
    widened = tokens.astype(jnp.float32)
    squares = by_axis(jnp.sum(widened * widened, axis=1), KV_TP)
    normed = collect((widened * gain_row.astype(jnp.float32)).astype(jnp.bfloat16), "tp", 1)
    return (normed, lax.rsqrt(squares / D + epsilon))


def half_mlp(tokens, gain_row, w_gate, w_up, w_down):
    widened = tokens.astype(jnp.float32)
    normed, factor = block_rows(tokens, gain_row)
    row_count = normed.shape[0]
    gate_term = lax.dot_general(
        w_gate, normed, (((0,), (1,)), ((), ())), preferred_element_type=jnp.float32
    )
    up_term = lax.dot_general(
        w_up, normed, (((0,), (1,)), ((), ())), preferred_element_type=jnp.float32
    )
    summed = sum_at_owner(jnp.concatenate([gate_term, up_term], axis=1).astype(jnp.bfloat16), KV, 0)
    gate_share = factor[None, :] * summed[:, :row_count]
    up_share = factor[None, :] * summed[:, row_count:]
    hidden_share = (jax.nn.silu(gate_share) * up_share).astype(jnp.bfloat16)
    hidden_cols = collect(hidden_share, KV, 0)
    partial_value = lax.dot_general(
        hidden_cols, w_down, (((0,), (0,)), ((), ())), preferred_element_type=jnp.float32
    )
    lowered = sum_at_owner(partial_value.astype(jnp.bfloat16), "tp", 1)
    return (widened + 0.5 * lowered).astype(jnp.bfloat16)


def on_device(
    tokens,
    gain_in,
    gate_in,
    up_in,
    down_in,
    gain_mix,
    w_query,
    w_key,
    w_value,
    w_gate,
    w_mixout,
    forget_rate,
    state_in,
    positions,
    gain_out,
    gate_out,
    up_out,
    down_out,
):
    after_first = half_mlp(tokens, gain_in, gate_in, up_in, down_in)
    widened = after_first.astype(jnp.float32)
    own_rows = state_in.shape[0]
    normed, factor_all = block_rows(after_first, gain_mix)
    head_count = w_query.shape[1] // DK
    weights = (w_query, w_key, w_value, w_gate)
    projected = sum_at_owner(
        jnp.concatenate(
            [jnp.dot(normed, weight, preferred_element_type=jnp.float32) for weight in weights],
            axis=1,
        ).astype(jnp.bfloat16),
        KV,
        0,
    )
    factor = lax.dynamic_slice_in_dim(factor_all, lax.axis_index(KV) * own_rows, own_rows)[:, None]
    rounded = lax.optimization_barrier((factor * projected).astype(jnp.bfloat16))
    scaled = rounded.astype(jnp.float32)
    bounds = [head_count * DK, 2 * head_count * DK, 2 * head_count * DK + head_count * DV]
    sections = jnp.split(scaled, bounds, axis=1)
    queries = rotate(sections[0].reshape(own_rows, head_count, DK), positions)
    key_rot = rotate(sections[1].reshape(own_rows, head_count, DK), positions) * DK ** (-0.5)
    values_now = sections[2].reshape(own_rows, head_count, DV)
    gates_now = sections[3].reshape(own_rows, head_count, DV)
    decays = jnp.exp(-forget_rate)
    carried = jnp.einsum("bhd,bhde->bhe", queries, state_in)
    present = jnp.sum(queries * key_rot, axis=-1, keepdims=True) * values_now
    retained = present + decays[None, :, None] * carried
    new_state = (
        decays[None, :, None, None] * state_in + key_rot[..., None] * values_now[..., None, :]
    )
    normed_heads = retained * lax.rsqrt(
        jnp.mean(retained * retained, axis=-1, keepdims=True) + epsilon
    )
    mixed = (
        (jax.nn.silu(gates_now) * normed_heads)
        .astype(jnp.bfloat16)
        .reshape(own_rows, head_count * DV)
    )
    head_terms = jnp.dot(
        lax.all_gather(mixed, KV, axis=0, tiled=True), w_mixout, preferred_element_type=jnp.float32
    )
    mixed_sum = sum_at_owner(head_terms.astype(jnp.bfloat16), "tp", 1)
    second = (widened + mixed_sum).astype(jnp.bfloat16)
    result = half_mlp(second, gain_out, gate_out, up_out, down_out)
    return (result, new_state)


def solution(mesh):
    split = Mesh(
        mesh.devices.reshape(mesh.shape["grp"], 8, 2, mesh.shape["tp"]),
        ("grp", "kv_0", "kv_1", "tp"),
    )
    placed = (
        P("grp", KV_TP),
        P(KV_TP),
        P(KV, "tp"),
        P(KV, "tp"),
        P("tp", KV),
        P(KV_TP),
        P(KV, "tp"),
        P(KV, "tp"),
        P(KV, "tp"),
        P(KV, "tp"),
        P("tp", KV),
        P("tp"),
        P(GRP_KV, "tp", None, None),
        P(GRP_KV),
        P(KV_TP),
        P(KV, "tp"),
        P(KV, "tp"),
        P("tp", KV),
    )
    return jax.shard_map(
        on_device,
        mesh=split,
        in_specs=placed,
        out_specs=(P("grp", KV_TP), P(GRP_KV, "tp", None, None)),
        check_vma=False,
    )
```

profile of v0, /device:TPU:513, one launch (start us, length us, event | category | flops | bytes accessed | tf_op | source)
XLA Modules:
  0.0 300.2 jit_solution(15824560088597087036)
XLA Ops:
  0.7 0.8 convert_element_type.93
  1.4 0.8 fusion.14
  2.2 14.9 %all_to_all.55 = bf16[8,128,32]{1,2,0:T(8,128)(2,1)S(1)} all-to-all(bf16[8,128,32]{1,2,0:T(8,128)(2,1)S(1)} %broadcast_in_dim.10), channel_id=1, replica_groups=mesh['grp'=2,'kv_0'=8,'kv_1'=2,'tp'=8] {'tp'}, dimensions={0} | all-to-all | bytes 131072 | tf_op jit(solution)/shard_map/all_to_all | solution.py:32
  18.0 0.9 pad_maximum_fusion
  18.9 19.8 %all-to-all-start.1 = ((bf16[16,86,256]{2,1,0:T(8,128)(2,1)}), bf16[16,86,256]{2,1,0:T(8,128)(2,1)S(1)}, u32[]{:S(2)}, u32[]{:S(2)}) async-start(bf16[16,86,256]{2,1,0:T(8,128)(2,1)} %pad_maximum_fusion), calls=%async_computation.1 | async-start | bytes 1441792 | tf_op jit(solution)/shard_map/all_to_all | solution.py:48
  38.7 26.2 %psum.63 = f32[128]{0:T(128)S(1)} all-reduce(f32[128]{0:T(128)S(1)} %get-tuple-element.10), channel_id=1, replica_groups=mesh['grp'=2,'kv_0'=8,'kv_1'=2,'tp'=8] {'kv_0'}, use_global_device_ids=true, to_apply=%region_1.0 | all-reduce | flops 128 | bytes 1024 | tf_op jit(solution)/shard_map/psum | solution.py:20
  64.9 5.5 %psum.64 = f32[128]{0:T(128)S(1)} all-reduce(f32[128]{0:T(128)S(1)} %psum.63), channel_id=1, replica_groups=mesh['grp'=2,'kv_0'=8,'kv_1'=2,'tp'=8] {'kv_1'}, use_global_device_ids=true, to_apply=%region_2.0 | all-reduce | flops 128 | bytes 1024 | tf_op jit(solution)/shard_map/psum | solution.py:20
  70.4 11.0 %psum.65 = f32[128]{0:T(128)S(1)} all-reduce(f32[128]{0:T(128)S(1)} %psum.64), channel_id=1, replica_groups=mesh['grp'=2,'kv_0'=8,'kv_1'=2,'tp'=8] {'tp'}, use_global_device_ids=true, to_apply=%region_3.0 | all-reduce | flops 128 | bytes 1024 | tf_op jit(solution)/shard_map/psum | solution.py:20
  81.6 23.6 %all_to_all.56 = bf16[16,86,128]{2,1,0:T(8,128)(2,1)S(1)} all-to-all(bf16[16,86,128]{2,1,0:T(8,128)(2,1)S(1)} %broadcast_in_dim.11), channel_id=1, replica_groups=mesh['grp'=2,'kv_0'=8,'kv_1'=2,'tp'=8] {'kv_0','kv_1'}, dimensions={0} | all-to-all | bytes 704512 | tf_op jit(solution)/shard_map/all_to_all | solution.py:32
  106.4 3.6 %all-to-all-start.3 = ((bf16[8,128,32]{1,2,0:T(8,128)(2,1)}), bf16[8,128,32]{1,2,0:T(8,128)(2,1)S(1)}, u32[]{:S(2)}, u32[]{:S(2)}) async-start(bf16[8,128,32]{1,2,0:T(8,128)(2,1)} %bitcast.6), calls=%async_computation.3 | async-start | bytes 131072 | tf_op jit(solution)/shard_map/all_to_all | solution.py:48
  110.0 8.1 %all-to-all-done.3 = bf16[8,128,32]{1,2,0:T(8,128)(2,1)S(1)} async-done(((bf16[8,128,32]{1,2,0:T(8,128)(2,1)}), bf16[8,128,32]{1,2,0:T(8,128)(2,1)S(1)}, u32[]{:S(2)}, u32[]{:S(2)}) %all-to-all-start.3) | async-done | bytes 65568 | tf_op jit(solution)/shard_map/all_to_all | solution.py:48
  118.2 9.5 %all_to_all.57 = bf16[8,128,32]{1,2,0:T(8,128)(2,1)S(1)} all-to-all(bf16[8,128,32]{1,2,0:T(8,128)(2,1)S(1)} %broadcast_in_dim.12), channel_id=1, replica_groups=mesh['grp'=2,'kv_0'=8,'kv_1'=2,'tp'=8] {'tp'}, dimensions={0} | all-to-all | bytes 131072 | tf_op jit(solution)/shard_map/all_to_all | solution.py:32
  129.6 5.2 %all-to-all-start.5 = ((bf16[16,8,768]{2,1,0:T(8,128)(2,1)}), bf16[16,8,768]{2,1,0:T(8,128)(2,1)S(1)}, u32[]{:S(2)}, u32[]{:S(2)}) async-start(bf16[16,8,768]{2,1,0:T(8,128)(2,1)} %pad_maximum_fusion.2), calls=%async_computation.5 | async-start | bytes 393216 | tf_op jit(solution)/shard_map/all_to_all | solution.py:48
  135.5 13.9 %psum.66 = f32[128]{0:T(128)S(1)} all-reduce(f32[128]{0:T(128)S(1)} %get-tuple-element.6), channel_id=1, replica_groups=mesh['grp'=2,'kv_0'=8,'kv_1'=2,'tp'=8] {'kv_0'}, use_global_device_ids=true, to_apply=%region_7.8 | all-reduce | flops 128 | bytes 1024 | tf_op jit(solution)/shard_map/psum | solution.py:20
  149.4 5.9 %psum.67 = f32[128]{0:T(128)S(1)} all-reduce(f32[128]{0:T(128)S(1)} %psum.66), channel_id=1, replica_groups=mesh['grp'=2,'kv_0'=8,'kv_1'=2,'tp'=8] {'kv_1'}, use_global_device_ids=true, to_apply=%region_8.9 | all-reduce | flops 128 | bytes 1024 | tf_op jit(solution)/shard_map/psum | solution.py:20
  155.3 11.0 %psum.68 = f32[128]{0:T(128)S(1)} all-reduce(f32[128]{0:T(128)S(1)} %psum.67), channel_id=1, replica_groups=mesh['grp'=2,'kv_0'=8,'kv_1'=2,'tp'=8] {'tp'}, use_global_device_ids=true, to_apply=%region_9.10 | all-reduce | flops 128 | bytes 1024 | tf_op jit(solution)/shard_map/psum | solution.py:20
  167.3 19.3 %all_gather.3 = bf16[128,256]{1,0:T(8,128)(2,1)S(1)} all-gather(bf16[8,256]{1,0:T(8,128)(2,1)S(1)} %multiply_convert_fusion.1), channel_id=1, replica_groups=mesh['grp'=2,'kv_0'=8,'kv_1'=2,'tp'=8] {'kv_0','kv_1'}, dimensions={0}, use_global_device_ids=true | all-gather | bytes 69632 | tf_op jit(solution)/shard_map/all_gather | solution.py:157
  187.5 3.6 %all-to-all-start.6 = ((bf16[8,128,32]{1,2,0:T(8,128)(2,1)}), bf16[8,128,32]{1,2,0:T(8,128)(2,1)S(1)}, u32[]{:S(2)}, u32[]{:S(2)}) async-start(bf16[8,128,32]{1,2,0:T(8,128)(2,1)} %bitcast.21), calls=%async_computation.6 | async-start | bytes 131072 | tf_op jit(solution)/shard_map/all_to_all | solution.py:48
  191.1 7.1 %all-to-all-done.6 = bf16[8,128,32]{1,2,0:T(8,128)(2,1)S(1)} async-done(((bf16[8,128,32]{1,2,0:T(8,128)(2,1)}), bf16[8,128,32]{1,2,0:T(8,128)(2,1)S(1)}, u32[]{:S(2)}, u32[]{:S(2)}) %all-to-all-start.6) | async-done | bytes 65568 | tf_op jit(solution)/shard_map/all_to_all | solution.py:48
  198.4 9.9 %all_to_all.58 = bf16[8,128,32]{1,2,0:T(8,128)(2,1)S(1)} all-to-all(bf16[8,128,32]{1,2,0:T(8,128)(2,1)S(1)} %broadcast_in_dim.13), channel_id=1, replica_groups=mesh['grp'=2,'kv_0'=8,'kv_1'=2,'tp'=8] {'tp'}, dimensions={0} | all-to-all | bytes 131072 | tf_op jit(solution)/shard_map/all_to_all | solution.py:32
  209.3 1.2 fusion.3
  210.6 0.9 pad_maximum_fusion.1
  211.6 8.0 %all-to-all-start.8 = ((bf16[16,86,256]{2,1,0:T(8,128)(2,1)}), bf16[16,86,256]{2,1,0:T(8,128)(2,1)S(1)}, u32[]{:S(2)}, u32[]{:S(2)}) async-start(bf16[16,86,256]{2,1,0:T(8,128)(2,1)} %pad_maximum_fusion.1), calls=%async_computation.8 | async-start | bytes 1441792 | tf_op jit(solution)/shard_map/all_to_all | solution.py:48
  219.6 25.9 %psum.69 = f32[128]{0:T(128)S(1)} all-reduce(f32[128]{0:T(128)S(1)} %get-tuple-element.2), channel_id=1, replica_groups=mesh['grp'=2,'kv_0'=8,'kv_1'=2,'tp'=8] {'kv_0'}, use_global_device_ids=true, to_apply=%region_15.16 | all-reduce | flops 128 | bytes 1024 | tf_op jit(solution)/shard_map/psum | solution.py:20
  245.5 5.5 %psum.70 = f32[128]{0:T(128)S(1)} all-reduce(f32[128]{0:T(128)S(1)} %psum.69), channel_id=1, replica_groups=mesh['grp'=2,'kv_0'=8,'kv_1'=2,'tp'=8] {'kv_1'}, use_global_device_ids=true, to_apply=%region_16.17 | all-reduce | flops 128 | bytes 1024 | tf_op jit(solution)/shard_map/psum | solution.py:20
  251.0 11.0 %psum.71 = f32[128]{0:T(128)S(1)} all-reduce(f32[128]{0:T(128)S(1)} %psum.70), channel_id=1, replica_groups=mesh['grp'=2,'kv_0'=8,'kv_1'=2,'tp'=8] {'tp'}, use_global_device_ids=true, to_apply=%region_17.18 | all-reduce | flops 128 | bytes 1024 | tf_op jit(solution)/shard_map/psum | solution.py:20
  262.1 0.8 broadcast_in_dim.14
  262.9 10.1 %all-to-all-start.9 = ((bf16[16,86,128]{2,1,0:T(8,128)(2,1)}), bf16[16,86,128]{2,1,0:T(8,128)(2,1)S(1)}, u32[]{:S(2)}, u32[]{:S(2)}) async-start(bf16[16,86,128]{2,1,0:T(8,128)(2,1)} %broadcast_in_dim.14), calls=%async_computation.9 | async-start | bytes 720896 | tf_op jit(solution)/shard_map/all_to_all | solution.py:32
  273.1 13.7 %all-to-all-done.9 = bf16[16,86,128]{2,1,0:T(8,128)(2,1)S(1)} async-done(((bf16[16,86,128]{2,1,0:T(8,128)(2,1)}), bf16[16,86,128]{2,1,0:T(8,128)(2,1)S(1)}, u32[]{:S(2)}, u32[]{:S(2)}) %all-to-all-start.9) | async-done | bytes 352288 | tf_op jit(solution)/shard_map/all_to_all | solution.py:32
  287.9 3.6 %all-to-all-start.10 = ((bf16[8,128,32]{1,2,0:T(8,128)(2,1)}), bf16[8,128,32]{1,2,0:T(8,128)(2,1)S(1)}, u32[]{:S(2)}, u32[]{:S(2)}) async-start(bf16[8,128,32]{1,2,0:T(8,128)(2,1)} %bitcast.28), calls=%async_computation.10 | async-start | bytes 131072 | tf_op jit(solution)/shard_map/all_to_all | solution.py:48
  291.5 1.2 multiply_add_fusion
  292.7 6.9 %all-to-all-done.10 = bf16[8,128,32]{1,2,0:T(8,128)(2,1)S(1)} async-done(((bf16[8,128,32]{1,2,0:T(8,128)(2,1)}), bf16[8,128,32]{1,2,0:T(8,128)(2,1)S(1)}, u32[]{:S(2)}, u32[]{:S(2)}) %all-to-all-start.10) | async-done | bytes 65568 | tf_op jit(solution)/shard_map/all_to_all | solution.py:48
  (95 shorter events, 9.3 us)
Async XLA Ops:
  0.6 16.5 %copy-start = (bf16[256,1376]{0,1:T(8,128)(2,1)S(1)}, bf16[256,1376]{0,1:T(8,128)(2,1)}, u32[]{:S(2)}) copy-start(bf16[256,1376]{0,1:T(8,128)(2,1)} %param.20) | copy-start | bytes 2113540
  0.6 16.9 %copy-start.2 = (bf16[256,1376]{0,1:T(8,128)(2,1)S(1)}, bf16[256,1376]{0,1:T(8,128)(2,1)}, u32[]{:S(2)}) copy-start(bf16[256,1376]{0,1:T(8,128)(2,1)} %param.21) | copy-start | bytes 2113540
  18.9 62.4 %all-to-all-start.1 = ((bf16[16,86,256]{2,1,0:T(8,128)(2,1)}), bf16[16,86,256]{2,1,0:T(8,128)(2,1)S(1)}, u32[]{:S(2)}, u32[]{:S(2)}) async-start(bf16[16,86,256]{2,1,0:T(8,128)(2,1)} %pad_maximum_fusion), calls=%async_computation.1 | async-start | bytes 1441792 | tf_op jit(solution)/shard_map/all_to_all | solution.py:48
  81.5 23.8 %copy-start.3 = (bf16[1376,256]{1,0:T(8,128)(2,1)S(1)}, bf16[1376,256]{1,0:T(8,128)(2,1)}, u32[]{:S(2)}) copy-start(bf16[1376,256]{1,0:T(8,128)(2,1)} %param.22) | copy-start | bytes 2113540
  105.2 4.8 %copy-start.14 = (bf16[32]{0:T(256)(128)(2,1)S(1)}, bf16[32]{0:T(256)(128)(2,1)}, u32[]{:S(2)}) copy-start(bf16[32]{0:T(256)(128)(2,1)} %param.23) | copy-start | bytes 196
  105.2 12.9 %copy-start.13 = (bf16[128,32]{0,1:T(8,128)(2,1)S(1)}, bf16[128,32]{0,1:T(8,128)(2,1)}, u32[]{:S(2)}) copy-start(bf16[128,32]{0,1:T(8,128)(2,1)} %param.18) | copy-start | bytes 24580
  105.3 22.9 %copy-start.11 = (bf16[256,128]{1,0:T(8,128)(2,1)S(1)}, bf16[256,128]{1,0:T(8,128)(2,1)}, u32[]{:S(2)}) copy-start(bf16[256,128]{1,0:T(8,128)(2,1)} %param.25) | copy-start | bytes 196612
  105.3 23.0 %copy-start.12 = (bf16[256,128]{1,0:T(8,128)(2,1)S(1)}, bf16[256,128]{1,0:T(8,128)(2,1)}, u32[]{:S(2)}) copy-start(bf16[256,128]{1,0:T(8,128)(2,1)} %param.24) | copy-start | bytes 196612
  105.7 22.8 %copy-start.8 = (bf16[256,256]{1,0:T(8,128)(2,1)S(1)}, bf16[256,256]{1,0:T(8,128)(2,1)}, u32[]{:S(2)}) copy-start(bf16[256,256]{1,0:T(8,128)(2,1)} %param.27) | copy-start | bytes 393220
  105.7 23.0 %copy-start.9 = (bf16[256,256]{1,0:T(8,128)(2,1)S(1)}, bf16[256,256]{1,0:T(8,128)(2,1)}, u32[]{:S(2)}) copy-start(bf16[256,256]{1,0:T(8,128)(2,1)} %param.26) | copy-start | bytes 393220
  106.4 11.7 %all-to-all-start.3 = ((bf16[8,128,32]{1,2,0:T(8,128)(2,1)}), bf16[8,128,32]{1,2,0:T(8,128)(2,1)S(1)}, u32[]{:S(2)}, u32[]{:S(2)}) async-start(bf16[8,128,32]{1,2,0:T(8,128)(2,1)} %bitcast.6), calls=%async_computation.3 | async-start | bytes 131072 | tf_op jit(solution)/shard_map/all_to_all | solution.py:48
  128.0 7.5 %copy-start.15 = (s32[8]{0:T(128)S(1)}, s32[8]{0:T(128)}, u32[]{:S(2)}) copy-start(s32[8]{0:T(128)} %param.31) | copy-start | bytes 100
  128.2 38.7 %copy-start.1 = (f32[8,1,128,256]{3,2,1,0:T(8,128)S(1)}, f32[8,1,128,256]{3,2,1,0:T(8,128)}, u32[]{:S(2)}) copy-start(f32[8,1,128,256]{3,2,1,0:T(8,128)} %param.30) | copy-start | bytes 3145732
  129.6 57.0 %copy-start.10 = (bf16[256,256]{1,0:T(8,128)(2,1)S(1)}, bf16[256,256]{1,0:T(8,128)(2,1)}, u32[]{:S(2)}) copy-start(bf16[256,256]{1,0:T(8,128)(2,1)} %param.28) | copy-start | bytes 393220
  129.6 36.8 %all-to-all-start.5 = ((bf16[16,8,768]{2,1,0:T(8,128)(2,1)}), bf16[16,8,768]{2,1,0:T(8,128)(2,1)S(1)}, u32[]{:S(2)}, u32[]{:S(2)}) async-start(bf16[16,8,768]{2,1,0:T(8,128)(2,1)} %pad_maximum_fusion.2), calls=%async_computation.5 | async-start | bytes 393216 | tf_op jit(solution)/shard_map/all_to_all | solution.py:48
  166.3 24.8 %copy-start.16 = (bf16[32]{0:T(256)(128)(2,1)S(1)}, bf16[32]{0:T(256)(128)(2,1)}, u32[]{:S(2)}) copy-start(bf16[32]{0:T(256)(128)(2,1)} %param.32) | copy-start | bytes 196
  166.6 42.3 %copy-start.4 = (bf16[256,1376]{0,1:T(8,128)(2,1)S(1)}, bf16[256,1376]{0,1:T(8,128)(2,1)}, u32[]{:S(2)}) copy-start(bf16[256,1376]{0,1:T(8,128)(2,1)} %param.33) | copy-start | bytes 2113540
  187.5 10.7 %all-to-all-start.6 = ((bf16[8,128,32]{1,2,0:T(8,128)(2,1)}), bf16[8,128,32]{1,2,0:T(8,128)(2,1)S(1)}, u32[]{:S(2)}, u32[]{:S(2)}) async-start(bf16[8,128,32]{1,2,0:T(8,128)(2,1)} %bitcast.21), calls=%async_computation.6 | async-start | bytes 131072 | tf_op jit(solution)/shard_map/all_to_all | solution.py:48
  198.3 11.1 %copy-start.5 = (bf16[256,1376]{0,1:T(8,128)(2,1)S(1)}, bf16[256,1376]{0,1:T(8,128)(2,1)}, u32[]{:S(2)}) copy-start(bf16[256,1376]{0,1:T(8,128)(2,1)} %param.34) | copy-start | bytes 2113540
  208.3 0.6 copy-start.7
  211.6 50.4 %all-to-all-start.8 = ((bf16[16,86,256]{2,1,0:T(8,128)(2,1)}), bf16[16,86,256]{2,1,0:T(8,128)(2,1)S(1)}, u32[]{:S(2)}, u32[]{:S(2)}) async-start(bf16[16,86,256]{2,1,0:T(8,128)(2,1)} %pad_maximum_fusion.1), calls=%async_computation.8 | async-start | bytes 1441792 | tf_op jit(solution)/shard_map/all_to_all | solution.py:48
  262.1 24.8 %copy-start.6 = (bf16[1376,256]{1,0:T(8,128)(2,1)S(1)}, bf16[1376,256]{1,0:T(8,128)(2,1)}, u32[]{:S(2)}) copy-start(bf16[1376,256]{1,0:T(8,128)(2,1)} %param.35) | copy-start | bytes 2113540
  262.9 23.8 %all-to-all-start.9 = ((bf16[16,86,128]{2,1,0:T(8,128)(2,1)}), bf16[16,86,128]{2,1,0:T(8,128)(2,1)S(1)}, u32[]{:S(2)}, u32[]{:S(2)}) async-start(bf16[16,86,128]{2,1,0:T(8,128)(2,1)} %broadcast_in_dim.14), calls=%async_computation.9 | async-start | bytes 720896 | tf_op jit(solution)/shard_map/all_to_all | solution.py:32
  287.9 11.7 %all-to-all-start.10 = ((bf16[8,128,32]{1,2,0:T(8,128)(2,1)}), bf16[8,128,32]{1,2,0:T(8,128)(2,1)S(1)}, u32[]{:S(2)}, u32[]{:S(2)}) async-start(bf16[8,128,32]{1,2,0:T(8,128)(2,1)} %bitcast.28), calls=%async_computation.10 | async-start | bytes 131072 | tf_op jit(solution)/shard_map/all_to_all | solution.py:48
where the time goes:
time: 301 us; the launch traced here: 300 us
  blocking collectives  193 us (64%)
  starting transfers between devices  53.7 us (18%)
  waiting for transfers between devices  35.8 us (12%)
  other arithmetic  7.2 us (2%)
  local copies, waits for them, and re-layouts  4.81 us (2%)
  matrix products  3.79 us (1%)
    psum x9, blocking collectives, by_axis(): value = lax.psum(value, axis)  116 us
    all_to_all x4, blocking collectives, sent_to_all(): lax.all_to_all(jnp.broadcast_to(value[None], (count, *value.shape)), axis...  57.9 us
    all_to_all x6, starting transfers between devices, sum_at_owner(): lax.all_to_all(tiles, axis, split_axis=0, concat_axis=0, tiled=True)  43.7 us
    all_to_all x6, waiting for transfers between devices, sum_at_owner(): lax.all_to_all(tiles, axis, split_axis=0, concat_axis=0, tiled=True)  22.2 us
    all_gather x1, blocking collectives, on_device(): lax.all_gather(mixed, KV, axis=0, tiled=True)  19.3 us
    all_to_all x1, waiting for transfers between devices, sent_to_all(): lax.all_to_all(jnp.broadcast_to(value[None], (count, *value.shape)), axis...  13.7 us
    all_to_all x1, starting transfers between devices, sent_to_all(): lax.all_to_all(jnp.broadcast_to(value[None], (count, *value.shape)), axis...  10.1 us
  transfers between devices with their start and end apart: 7, of which 4 were waited for; matrix products, arithmetic and copies ran while one was open for 0% of the time, Pallas kernels for 0%

commit v1 on v0

v1 whole, which is shorter than its diff:
```python
import functools
import math

import jax
import jax.numpy as jnp
from jax import lax
from jax.experimental import pallas as pl
from jax.experimental.pallas import tpu as pltpu
from jax.sharding import PartitionSpec as P

EPS = 1e-06
BASE = 10000.0
MESH = pl.DeviceIdType.MESH
F32 = jnp.float32
BF16 = jnp.bfloat16


def far_first(n):
    return sorted(range(1, n), key=lambda j: -min(j, n - j))


def near_first(n):
    return sorted(range(1, n), key=lambda j: min(j, n - j))


def widths(total, cut):
    edges = [0, *[c for c in cut if c < total], total]
    return list(zip(edges[:-1], edges[1:]))


def tiles(first, last, step=256):
    return [(at, min(at + step, last)) for at in range(first, last, step)]


def kernel(dims, tokens, gain_in, gain_mix, gain_out, forget, positions,
           gate_in, up_in, down_in, w_query, w_key, w_value, w_gate, w_mix, state,
           gate_out, up_out, down_out,
           result, key_out, value_out, *scratch):
    NT, NY, NK, R, OWN, C, c, FF, DK, DV, D, mlp_pieces, qkv_pieces = dims
    (tok_v, gains_v, gi_v, ui_v, di_v, wq_v, wk_v, wv_v, wg_v, wm_v, st_v, go_v, uo_v, do_v, load_sem,
     xall, ss_src, ssx, ss_k, ss_b, ss_c, ssy, fac,
     part_m, sib_m, red_m, recv_m, part_q, sib_q, red_q, recv_q,
     hall, mall, px, rx, oT,
     ax_s, axs_s, sib_s, ssb_s, y_s, ssy_s, ag_s, agf_s, rx_s,
     ax_r, axs_r, sib_r, ssb_r, y_r, ssy_r, ag_r, agf_r, rx_r) = scratch

    t = lax.axis_index("tp")
    k = lax.axis_index("kv")
    core = lax.rem(k, 2)
    y = lax.div(k, 2)
    sibling = {"kv": k + 1 - 2 * core}

    def at_t(j):
        return lax.rem(t + j, NT)

    def at_y(j):
        return lax.rem(y + j, NY)

    def chip(j):
        return {"kv": 2 * at_y(j) + core}

    loads = []
    pairs = [(tokens, tok_v), (gain_in, gains_v.at[0]), (gain_mix, gains_v.at[1]), (gain_out, gains_v.at[2]),
             (gate_in, gi_v), (up_in, ui_v), (w_query, wq_v), (w_key, wk_v), (w_value, wv_v), (w_gate, wg_v),
             (down_in, di_v), (w_mix, wm_v), (state, st_v), (gate_out, go_v), (up_out, uo_v), (down_out, do_v)]
    for i, (src, dst) in enumerate(pairs):
        copy = pltpu.make_async_copy(src, dst, load_sem.at[i])
        copy.start()
        loads.append(copy)

    barrier = pltpu.get_barrier_semaphore()
    pl.semaphore_signal(barrier, inc=1, device_id=sibling, device_id_type=MESH)
    for j in far_first(NT):
        pl.semaphore_signal(barrier, inc=1, device_id={"tp": at_t(j)}, device_id_type=MESH)
    for j in far_first(NY):
        pl.semaphore_signal(barrier, inc=1, device_id=chip(j), device_id_type=MESH)

    for i in range(4):
        loads[i].wait()
    tok = tok_v[...].astype(F32)

    def column(i):
        row = jnp.broadcast_to(gains_v[i].astype(F32), (R, c))
        return row.T

    resid = tok.T
    pl.semaphore_wait(barrier, 1 + (NT - 1) + (NY - 1))

    pending = {}

    def remote(src, dst, ssem, rsem, device):
        return pltpu.make_async_remote_copy(src_ref=src, dst_ref=dst, send_sem=ssem, recv_sem=rsem,
                                            device_id=device, device_id_type=MESH)

    def flush(kind):
        for copy in pending.pop(kind, []):
            copy.wait_send()

    def gather_x(s, normed, squares):
        flush("ax")
        xall[s, t] = normed
        ss_src[s] = squares
        copies, small = [], []
        for j in far_first(NT):
            copy = remote(xall.at[s, t], xall.at[s, t], ax_s.at[j], ax_r.at[s, NT - j], {"tp": at_t(j)})
            copy.start()
            copies.append(copy)
        for j in far_first(NT):
            copy = remote(ss_src.at[s], ssx.at[s, NT - j], axs_s.at[j], axs_r.at[s, NT - j], {"tp": at_t(j)})
            copy.start()
            small.append(copy)
        for j in near_first(NT):
            remote(xall.at[s, t], xall.at[s, t], ax_s.at[j], ax_r.at[s, j], {"tp": at_t(j)}).wait_recv()
        pending["ax"] = copies + small
        whole = xall[s].astype(F32).reshape(C, R)
        return whole.T.astype(BF16)

    def squares_of_block(s, own):
        total = own
        for j in near_first(NT):
            remote(ss_src.at[s], ssx.at[s, j], axs_s.at[j], axs_r.at[s, j], {"tp": at_t(j)}).wait_recv()
            total = total + ssx[s, j]
        return total

    def scatter_y(s, pieces, compute, part, sib, red, recv, own_squares, first_piece):
        flush("y")
        copies = []
        for p in range(len(pieces)):
            compute(p)
            copy = remote(part[p].at[1 - core], sib[p], sib_s.at[p], sib_r.at[s, p], sibling)
            copy.start()
            copies.append(copy)
        block = squares_of_block(s, own_squares)
        ss_k[s] = block
        copy = remote(ss_k.at[s], ss_b.at[s], ssb_s.at[0], ssb_r.at[s], sibling)
        copy.start()
        copies.append(copy)
        for p in range(len(pieces)):
            remote(part[p].at[1 - core], sib[p], sib_s.at[p], sib_r.at[s, p], sibling).wait_recv()
            late = None
            for j in far_first(NY) + [0]:
                yd = at_y(j)
                red[p][yd] = (part[p][core, yd].astype(F32) + sib[p][yd].astype(F32)).astype(BF16)
                if late is not None:
                    late.start()
                    copies.append(late)
                late = None
                if j:
                    late = remote(red[p].at[yd], recv[p].at[NY - j], y_s.at[p, j], y_r.at[s, p, NY - j], chip(j))
        remote(ss_k.at[s], ss_b.at[s], ssb_s.at[0], ssb_r.at[s], sibling).wait_recv()
        chip_sum = block + ss_b[s]
        ss_c[s] = chip_sum
        for j in far_first(NY):
            copy = remote(ss_c.at[s], ssy.at[s, NY - j], ssy_s.at[j], ssy_r.at[s, NY - j], chip(j))
            copy.start()
            copies.append(copy)
        pending["y"] = copies
        total = chip_sum
        for j in near_first(NY):
            remote(ss_c.at[s], ssy.at[s, j], ssy_s.at[j], ssy_r.at[s, j], chip(j)).wait_recv()
            total = total + ssy[s, j]
        wide = jnp.broadcast_to(total, (128, R)).T
        fac[s] = lax.rsqrt(wide / D + EPS)
        factor = fac[s, pl.ds(pl.multiple_of(k * OWN, OWN), OWN), :][:, :1]
        sums = []
        for p in range(len(pieces)):
            acc = red[p][y].astype(F32)
            for j in near_first(NY):
                remote(red[p].at[y], recv[p].at[j], y_s.at[p, j], y_r.at[s, p, j], chip(j)).wait_recv()
                acc = acc + recv[p][j].astype(F32)
            sums.append(acc)
        return sums, factor

    def gather_y(s, buf):
        flush("ag")
        copies = []
        copy = remote(buf.at[k], buf.at[k], agf_s.at[0], agf_r.at[s, 0], sibling)
        copy.start()
        copies.append(copy)
        for j in far_first(NY):
            copy = remote(buf.at[k], buf.at[k], ag_s.at[j], ag_r.at[s, NY - j], chip(j))
            copy.start()
            copies.append(copy)
        for j in near_first(NY):
            slot = 2 * at_y(j) + core
            remote(buf.at[slot], buf.at[slot], ag_s.at[j], ag_r.at[s, j], chip(j)).wait_recv()
            copy = remote(buf.at[slot], buf.at[slot], agf_s.at[j], agf_r.at[s, j], sibling)
            copy.start()
            copies.append(copy)
        for j in [0] + near_first(NY):
            slot = 2 * at_y(j) + 1 - core
            remote(buf.at[slot], buf.at[slot], agf_s.at[j], agf_r.at[s, j], sibling).wait_recv()
        pending["ag"] = copies

    def scatter_x(s, product):
        flush("rx")
        px[s] = product.T.reshape(NT, c, R).astype(BF16)
        copies = []
        for j in far_first(NT):
            copy = remote(px.at[s, at_t(j)], rx.at[s, NT - j], rx_s.at[j], rx_r.at[s, NT - j], {"tp": at_t(j)})
            copy.start()
            copies.append(copy)
        pending["rx"] = copies
        total = px[s, t].astype(F32)
        for j in near_first(NT):
            remote(px.at[s, at_t(j)], rx.at[s, j], rx_s.at[j], rx_r.at[s, j], {"tp": at_t(j)}).wait_recv()
            total = total + rx[s, j].astype(F32)
        return total

    def half_mlp(s, resid, gain, gate, up, down, waits):
        squares = jnp.sum(resid * resid, axis=0, keepdims=True)
        normed = gather_x(s, (resid * gain).astype(BF16), squares)
        for i in waits[:2]:
            loads[i].wait()

        def compute(p):
            first, last = mlp_pieces[p]
            for lo, hi in tiles(first, last):
                g = jnp.dot(normed, gate[:, lo:hi], preferred_element_type=F32)
                u = jnp.dot(normed, up[:, lo:hi], preferred_element_type=F32)
                for kk in range(NK):
                    rows = slice(OWN * kk, OWN * kk + OWN)
                    part_m[p][kk % 2, kk // 2, :, lo - first:hi - first] = jnp.concatenate(
                        [g[rows], u[rows]], axis=0).astype(BF16)

        sums, factor = scatter_y(s, mlp_pieces, compute, part_m, sib_m, red_m, [r.at[s // 2] for r in recv_m],
                                 squares, 0)
        for (first, last), acc in zip(mlp_pieces, sums):
            g = factor * acc[:OWN]
            u = factor * acc[OWN:]
            hall[s // 2, k, :, first:last] = (g / (1.0 + jnp.exp(-g)) * u).astype(BF16)
        gather_y(s, hall.at[s // 2])
        loads[waits[2]].wait()
        hidden = hall[s // 2].astype(F32).reshape(R, FF).astype(BF16)
        product = jnp.dot(hidden, down[...], preferred_element_type=F32)
        return resid + 0.5 * scatter_x(s, product)

    resid = half_mlp(0, resid, column(0), gi_v, ui_v, di_v, (4, 5, 10)).astype(BF16).astype(F32)

    squares = jnp.sum(resid * resid, axis=0, keepdims=True)
    normed = gather_x(1, (resid * column(1)).astype(BF16), squares)
    for i in (6, 7, 8, 9):
        loads[i].wait()

    def compute_qkv(p):
        q = jnp.dot(normed, wq_v[...], preferred_element_type=F32)
        kk_ = jnp.dot(normed, wk_v[...], preferred_element_type=F32)
        v = jnp.dot(normed, wv_v[...], preferred_element_type=F32)
        g = jnp.dot(normed, wg_v[...], preferred_element_type=F32)
        half = DV // 2
        top = [q, kk_, v[:, :half]]
        low = [v[:, half:], g[:, :half], g[:, half:]]
        for i in range(3):
            for kk in range(NK):
                rows = slice(OWN * kk, OWN * kk + OWN)
                part_q[0][kk % 2, kk // 2, :, DK * i:DK * i + DK] = jnp.concatenate(
                    [top[i][rows], low[i][rows]], axis=0).astype(BF16)

    sums, factor = scatter_y(1, qkv_pieces, compute_qkv, part_q, sib_q, red_q, recv_q, squares, 0)
    acc = (jnp.concatenate([factor, factor], axis=0) * sums[0]).astype(BF16).astype(F32)
    q, key = acc[:OWN, :DK], acc[:OWN, DK:2 * DK]
    value = jnp.concatenate([acc[:OWN, 2 * DK:], acc[OWN:, :DK]], axis=1)
    out_gate = acc[OWN:, DK:]

    row = lax.broadcasted_iota(jnp.int32, (OWN, DK), 0)
    lane = lax.broadcasted_iota(jnp.int32, (OWN, DK), 1)
    place = jnp.zeros((OWN, DK), F32)
    for r in range(OWN):
        place = jnp.where(row == r, positions[r].astype(F32), place)
    half = DK // 2
    pair = jnp.where(lane < half, lane, lane - half).astype(F32)
    angle = place * jnp.exp(pair * (-2.0 * math.log(BASE) / DK))
    cosine = jnp.cos(angle)
    sine = jnp.where(lane < half, -jnp.sin(angle), jnp.sin(angle))

    def rotate(v):
        return v * cosine + jnp.concatenate([v[:, half:], v[:, :half]], axis=1) * sine

    q = rotate(q)
    key = rotate(key) * DK ** (-0.5)
    decay = jnp.exp(jnp.broadcast_to(-forget[0], (1, DV)))
    q_col = q.T
    loads[12].wait()
    carried = jnp.concatenate(
        [jnp.sum(st_v[b] * q_col[:, b:b + 1], axis=0, keepdims=True) for b in range(OWN)], axis=0)
    retained = jnp.sum(q * key, axis=1, keepdims=True) * value + decay * carried
    scaled = retained * lax.rsqrt(jnp.mean(retained * retained, axis=1, keepdims=True) + EPS)
    mall[k] = (out_gate / (1.0 + jnp.exp(-out_gate)) * scaled).astype(BF16)
    key_out[...] = key
    value_out[...] = value
    gather_y(1, mall)
    loads[11].wait()
    mixed = mall[...].astype(F32).reshape(R, DV).astype(BF16)
    product = jnp.dot(mixed, wm_v[...], preferred_element_type=F32)
    resid = (resid + scatter_x(1, product)).astype(BF16).astype(F32)

    out = half_mlp(2, resid, column(2), go_v, uo_v, do_v, (13, 14, 15))
    result[...] = out.T.astype(BF16)
    for kind in ("ax", "y", "ag", "rx"):
        flush(kind)


def on_device(tokens, gain_in, gate_in, up_in, down_in, gain_mix, w_query, w_key, w_value, w_gate,
              w_mixout, forget_rate, state_in, positions, gain_out, gate_out, up_out, down_out):
    NT = lax.axis_size("tp")
    NK = lax.axis_size("kv")
    NY = NK // 2
    R, c = tokens.shape
    C, FF = gate_in.shape
    OWN, _, DK, DV = state_in.shape
    D = C * NK
    mlp_pieces = widths(FF, (768,))
    qkv_pieces = [(0, 3 * DK)]
    dims = (NT, NY, NK, R, OWN, C, c, FF, DK, DV, D, mlp_pieces, qkv_pieces)

    def exchange(pieces, calls):
        wide = [last - first for first, last in pieces]
        return (
            [pltpu.VMEM((2, NY, 2 * OWN, w), BF16) for w in wide],
            [pltpu.VMEM((NY, 2 * OWN, w), BF16) for w in wide],
            [pltpu.VMEM((NY, 2 * OWN, w), BF16) for w in wide],
            [pltpu.VMEM((*calls, NY, 2 * OWN, w), BF16) for w in wide],
        )

    dma = pltpu.SemaphoreType.DMA
    n_p = len(mlp_pieces)
    scratch = [
        pltpu.VMEM((R, c), BF16), pltpu.VMEM((3, 1, c), BF16),
        pltpu.VMEM((C, FF), BF16), pltpu.VMEM((C, FF), BF16), pltpu.VMEM((FF, C), BF16),
        pltpu.VMEM((C, DK), BF16), pltpu.VMEM((C, DK), BF16), pltpu.VMEM((C, DV), BF16), pltpu.VMEM((C, DV), BF16),
        pltpu.VMEM((DV, C), BF16), pltpu.VMEM((OWN, DK, DV), F32),
        pltpu.VMEM((C, FF), BF16), pltpu.VMEM((C, FF), BF16), pltpu.VMEM((FF, C), BF16),
        dma((16,)),
        pltpu.VMEM((3, NT, c, R), BF16), pltpu.VMEM((3, 1, R), F32), pltpu.VMEM((3, NT, 1, R), F32),
        pltpu.VMEM((3, 1, R), F32), pltpu.VMEM((3, 1, R), F32), pltpu.VMEM((3, 1, R), F32),
        pltpu.VMEM((3, NY, 1, R), F32), pltpu.VMEM((3, R, 128), F32),
        *exchange(mlp_pieces, (2,)),
        *exchange(qkv_pieces, ()),
        pltpu.VMEM((2, NK, OWN, FF), BF16), pltpu.VMEM((NK, OWN, DV), BF16),
        pltpu.VMEM((3, NT, c, R), BF16), pltpu.VMEM((3, NT, c, R), BF16), pltpu.VMEM((c, R), F32),
        dma((NT,)), dma((NT,)), dma((n_p,)), dma((1,)), dma((n_p, NY)), dma((NY,)), dma((NY,)), dma((NY,)), dma((NT,)),
        dma((3, NT)), dma((3, NT)), dma((3, n_p)), dma((3,)), dma((3, n_p, NY)), dma((3, NY)), dma((3, NY)),
        dma((3, NY)), dma((3, NT)),
    ]
    smem = pl.BlockSpec(memory_space=pltpu.SMEM)
    hbm = pl.BlockSpec(memory_space=pl.ANY)
    vmem = pl.BlockSpec(memory_space=pltpu.VMEM)
    result, key, value = pl.pallas_call(
        functools.partial(kernel, dims),
        out_shape=(jax.ShapeDtypeStruct((R, c), BF16), jax.ShapeDtypeStruct((OWN, DK), F32),
                   jax.ShapeDtypeStruct((OWN, DV), F32)),
        in_specs=[hbm] * 4 + [smem] * 2 + [hbm] * 12,
        out_specs=(vmem, vmem, vmem),
        scratch_shapes=scratch,
        compiler_params=pltpu.CompilerParams(collective_id=0, has_side_effects=True,
                                             vmem_limit_bytes=40 * 1024 * 1024),
        name="layer_step",
    )(tokens, gain_in[None], gain_mix[None], gain_out[None], forget_rate, positions,
      gate_in, up_in, down_in, w_query, w_key, w_value, w_gate, w_mixout, state_in.reshape(OWN, DK, DV), gate_out, up_out, down_out)
    decay = jnp.exp(-forget_rate)
    new_state = decay[None, :, None, None] * state_in + key[:, None, :, None] * value[:, None, None, :]
    return result, new_state


KV_TP = ("kv", "tp")


def solution(mesh):
    feature, wide, tall = P(KV_TP), P("kv", "tp"), P("tp", "kv")
    state = P(("grp", "kv"), "tp", None, None)
    placed = (P("grp", KV_TP), feature, wide, wide, tall, feature, wide, wide, wide, wide, tall, P("tp"), state,
              P(("grp", "kv")), feature, wide, wide, tall)
    return jax.shard_map(on_device, mesh=mesh, in_specs=placed, out_specs=(P("grp", KV_TP), state), check_vma=False)
```

time: 301 us -> 126 us (0.42)
  blocking collectives: 193 us -> 0 us
  Pallas kernels: 0 us -> 110 us
  starting transfers between devices: 53.7 us -> 0 us
  waiting for transfers between devices: 35.8 us -> 0 us
  local copies, waits for them, and re-layouts: 4.81 us -> 13 us
  other arithmetic: 7.2 us -> 1.18 us
  matrix products: 3.79 us -> 0 us
    psum x9 -> x0, blocking collectives: 116 us -> none  [by_axis(): value = lax.psum(value, axis)]
    pallas_call x0 -> x1, Pallas kernels: none -> 110 us  [on_device(): pl.pallas_call(functools.partial(kernel, dims), out_shape=(jax.ShapeDtype...]
    all_to_all x4 -> x0, blocking collectives: 57.9 us -> none  [sent_to_all(): lax.all_to_all(jnp.broadcast_to(value[None], (count, *value.shape)), axis...]
    all_to_all x7 -> x0, starting transfers between devices: 53.7 us -> none  [the longest x6 43.7 us: sum_at_owner(): lax.all_to_all(tiles, axis, split_axis=0, concat_axis=0, tiled=True)]
    all_to_all x7 -> x0, waiting for transfers between devices: 35.8 us -> none  [the longest x6 22.2 us: sum_at_owner(): lax.all_to_all(tiles, axis, split_axis=0, concat_axis=0, tiled=True)]
    all_gather x1 -> x0, blocking collectives: 19.3 us -> none  [on_device(): lax.all_gather(mixed, KV, axis=0, tiled=True)]
    unnamed x34 -> x36, local copies, waits for them, and re-layouts: 0.72 us -> 13 us
    dot_general x12 -> x0, matrix products: 3.79 us -> none  [the longest x2 1.51 us: half_mlp(): lax.dot_general(w_up, normed, (((0,), (1,)), ((), ())), preferred_element...]
  transfers between devices with their start and end apart: 7 -> 0, of which waited for: 4 -> 0; matrix products, arithmetic and copies ran while one was open for 0% -> 0% of each run, Pallas kernels for 0% -> 0%
where the time goes in v1:
time: 126 us
  Pallas kernels  110 us (87%)
  local copies, waits for them, and re-layouts  13 us (10%)
  between operations  1.45 us (1%)
    pallas_call x1, Pallas kernels, on_device(): pl.pallas_call(functools.partial(kernel, dims), out_shape=(jax.ShapeDtype...  110 us
    unnamed x36, local copies, waits for them, and re-layouts  13 us

profile of v1, /device:TPU:513, one launch (start us, length us, event | category | flops | bytes accessed | tf_op | source)
XLA Modules:
  0.0 126.0 jit_solution(12823680462141056686)
XLA Ops:
  1.3 0.0 copy-start.13
  1.3 1.5 %copy.21.gate_in = bf16[256,1376]{1,0:T(8,128)(2,1)S(1)} copy(bf16[256,1376]{0,1:T(8,128)(2,1)} %param.20) | data formatting | bytes 1409024 | tf_op args[2]
  2.8 0.0 copy-done.13
  2.8 0.3 copy.22.up_in
  3.2 1.4 %copy.23.gate_out = bf16[256,1376]{1,0:T(8,128)(2,1)S(1)} copy(bf16[256,1376]{0,1:T(8,128)(2,1)} %param.33) | data formatting | bytes 1409024 | tf_op args[15]
  4.6 0.0 copy-start.14
  4.6 0.0 copy-start
  4.6 0.0 copy-start.4
  4.6 0.0 copy-start.5
  4.6 0.0 copy-start.12
  4.7 2.3 %copy.24.up_out = bf16[256,1376]{1,0:T(8,128)(2,1)} copy(bf16[256,1376]{0,1:T(8,128)(2,1)} %param.34) | data formatting | bytes 1409024 | tf_op args[16]
  7.0 0.0 copy-done.14
  7.0 0.1 copy.20.tokens
  7.1 0.0 copy-start.9
  7.1 0.0 copy-start.10
  7.1 0.0 copy-start.11
  7.1 0.0 copy-done
  7.2 0.0 copy-done.4
  7.2 0.0 copy-done.5
  7.2 0.0 copy-done.12
  7.2 0.6 copy-done.9
  7.8 0.0 copy-done.10
  7.8 0.0 copy-done.11
  7.8 1.1 copy-done.1
  8.9 1.1 copy-done.2
  10.0 1.1 copy-done.3
  11.1 0.9 copy-done.6
  12.0 0.8 copy-done.7
  12.9 0.8 copy-done.8
  13.7 110.4 %layer_step.1 = (bf16[128,32]{1,0:T(8,128)(2,1)S(1)}, f32[8,128]{1,0:T(8,128)S(1)}, f32[8,256]{1,0:T(8,128)S(1)}) custom-call(bf16[128,32]{1,0:T(8,128)(2,1)S(1)} %copy.20.tokens, bf16[1,32]{1,0:T(2,128)(2,1)S(1)} %bitcast.6, bf16[1,32]{1,0:T(2,128)(2,1)S(1)} %bitcast.7, bf16[1,32]{1,0:T(2,128)(2,1)S(1)} %bitcast.8, f32[1]{0:T(128)S(6)} %copy.26.forget, ...), custom_call_target="tpu_custom_call" | custom-call | tf_op jit(solution)/shard_map/layer_step/pallas_call | solution.py:348
  124.2 1.2 multiply_add_fusion
  125.3 0.7 copy.25
  (6 shorter events, 0.0 us)
Async XLA Ops:
  1.3 1.5 %copy-start.13 = (bf16[256,1376]{0,1:T(8,128)(2,1)S(1)}, bf16[256,1376]{0,1:T(8,128)(2,1)}, u32[]{:S(2)}) copy-start(bf16[256,1376]{0,1:T(8,128)(2,1)} %param.21) | copy-start | bytes 2113540
  4.6 2.4 %copy-start.14 = (bf16[128,32]{0,1:T(8,128)(2,1)S(1)}, bf16[128,32]{0,1:T(8,128)(2,1)}, u32[]{:S(2)}) copy-start(bf16[128,32]{0,1:T(8,128)(2,1)} %param.18) | copy-start | bytes 24580
  4.6 2.5 %copy-start = (f32[8,1,128,256]{3,2,1,0:T(8,128)S(1)}, f32[8,1,128,256]{3,2,1,0:T(8,128)}, u32[]{:S(2)}) copy-start(f32[8,1,128,256]{3,2,1,0:T(8,128)} %param.30) | copy-start | bytes 3145732
  4.6 2.5 %copy-start.4 = (bf16[256,256]{1,0:T(8,128)(2,1)S(1)}, bf16[256,256]{1,0:T(8,128)(2,1)}, u32[]{:S(2)}) copy-start(bf16[256,256]{1,0:T(8,128)(2,1)} %w_value.1) | copy-start | bytes 393220
  4.6 2.5 %copy-start.5 = (bf16[256,256]{1,0:T(8,128)(2,1)S(1)}, bf16[256,256]{1,0:T(8,128)(2,1)}, u32[]{:S(2)}) copy-start(bf16[256,256]{1,0:T(8,128)(2,1)} %w_gate.1) | copy-start | bytes 393220
  4.6 2.5 %copy-start.12 = (s32[8]{0:T(128)S(1)}, s32[8]{0:T(128)}, u32[]{:S(2)}) copy-start(s32[8]{0:T(128)} %positions.1) | copy-start | bytes 100
  7.1 0.7 copy-start.9
  7.1 0.7 copy-start.10
  7.1 0.7 copy-start.11
  7.8 1.1 copy-start.1
  8.9 1.1 copy-start.2
  10.0 1.1 copy-start.3
  11.1 0.9 copy-start.6
  12.0 0.8 copy-start.7
  12.9 0.8 copy-start.8

commit v2 on v1

--- a/solution.py
+++ b/solution.py
@@ -77,13 +77,11 @@
 
     for i in range(4):
         loads[i].wait()
-    tok = tok_v[...].astype(F32)
-
     def column(i):
         row = jnp.broadcast_to(gains_v[i].astype(F32), (R, c))
         return row.T
 
-    resid = tok.T
+    resid = tok_v[...].astype(F32)
     pl.semaphore_wait(barrier, 1 + (NT - 1) + (NY - 1))
 
     pending = {}
@@ -216,8 +214,8 @@
         def compute(p):
             first, last = mlp_pieces[p]
             for lo, hi in tiles(first, last):
-                g = jnp.dot(normed, gate[:, lo:hi], preferred_element_type=F32)
-                u = jnp.dot(normed, up[:, lo:hi], preferred_element_type=F32)
+                g = lax.dot_general(normed, gate[lo:hi], (((1,), (1,)), ((), ())), preferred_element_type=F32)
+                u = lax.dot_general(normed, up[lo:hi], (((1,), (1,)), ((), ())), preferred_element_type=F32)
                 for kk in range(NK):
                     rows = slice(OWN * kk, OWN * kk + OWN)
                     part_m[p][kk % 2, kk // 2, :, lo - first:hi - first] = jnp.concatenate(
@@ -295,7 +293,7 @@
     resid = (resid + scatter_x(1, product)).astype(BF16).astype(F32)
 
     out = half_mlp(2, resid, column(2), go_v, uo_v, do_v, (13, 14, 15))
-    result[...] = out.T.astype(BF16)
+    result[...] = out.astype(BF16)
     for kind in ("ax", "y", "ag", "rx"):
         flush(kind)
 
@@ -325,11 +323,11 @@
     dma = pltpu.SemaphoreType.DMA
     n_p = len(mlp_pieces)
     scratch = [
-        pltpu.VMEM((R, c), BF16), pltpu.VMEM((3, 1, c), BF16),
-        pltpu.VMEM((C, FF), BF16), pltpu.VMEM((C, FF), BF16), pltpu.VMEM((FF, C), BF16),
+        pltpu.VMEM((c, R), BF16), pltpu.VMEM((3, 1, c), BF16),
+        pltpu.VMEM((FF, C), BF16), pltpu.VMEM((FF, C), BF16), pltpu.VMEM((FF, C), BF16),
         pltpu.VMEM((C, DK), BF16), pltpu.VMEM((C, DK), BF16), pltpu.VMEM((C, DV), BF16), pltpu.VMEM((C, DV), BF16),
         pltpu.VMEM((DV, C), BF16), pltpu.VMEM((OWN, DK, DV), F32),
-        pltpu.VMEM((C, FF), BF16), pltpu.VMEM((C, FF), BF16), pltpu.VMEM((FF, C), BF16),
+        pltpu.VMEM((FF, C), BF16), pltpu.VMEM((FF, C), BF16), pltpu.VMEM((FF, C), BF16),
         dma((16,)),
         pltpu.VMEM((3, NT, c, R), BF16), pltpu.VMEM((3, 1, R), F32), pltpu.VMEM((3, NT, 1, R), F32),
         pltpu.VMEM((3, 1, R), F32), pltpu.VMEM((3, 1, R), F32), pltpu.VMEM((3, 1, R), F32),
@@ -347,19 +345,20 @@
     vmem = pl.BlockSpec(memory_space=pltpu.VMEM)
     result, key, value = pl.pallas_call(
         functools.partial(kernel, dims),
-        out_shape=(jax.ShapeDtypeStruct((R, c), BF16), jax.ShapeDtypeStruct((OWN, DK), F32),
+        out_shape=(jax.ShapeDtypeStruct((c, R), BF16), jax.ShapeDtypeStruct((OWN, DK), F32),
                    jax.ShapeDtypeStruct((OWN, DV), F32)),
         in_specs=[hbm] * 4 + [smem] * 2 + [hbm] * 12,
         out_specs=(vmem, vmem, vmem),
         scratch_shapes=scratch,
         compiler_params=pltpu.CompilerParams(collective_id=0, has_side_effects=True,
-                                             vmem_limit_bytes=40 * 1024 * 1024),
+                                             vmem_limit_bytes=67043328),
         name="layer_step",
-    )(tokens, gain_in[None], gain_mix[None], gain_out[None], forget_rate, positions,
-      gate_in, up_in, down_in, w_query, w_key, w_value, w_gate, w_mixout, state_in.reshape(OWN, DK, DV), gate_out, up_out, down_out)
+    )(tokens.T, gain_in[None], gain_mix[None], gain_out[None], forget_rate, positions,
+      gate_in.T, up_in.T, down_in, w_query, w_key, w_value, w_gate, w_mixout, state_in.reshape(OWN, DK, DV),
+      gate_out.T, up_out.T, down_out)
     decay = jnp.exp(-forget_rate)
     new_state = decay[None, :, None, None] * state_in + key[:, None, :, None] * value[:, None, None, :]
-    return result, new_state
+    return result.T, new_state
 
 
 KV_TP = ("kv", "tp")

time: 126 us -> 115 us (0.913)
  local copies, waits for them, and re-layouts: 13 us -> 1.27 us
    unnamed x36 -> x5, local copies, waits for them, and re-layouts: 13 us -> 1.27 us
where the time goes in v2:
time: 115 us
  Pallas kernels  110 us (96%)
  other arithmetic  2.41 us (2%)
  between operations  1.34 us (1%)
  local copies, waits for them, and re-layouts  1.27 us (1%)
    pallas_call x1, Pallas kernels, on_device(): pl.pallas_call(functools.partial(kernel, dims), out_shape=(jax.ShapeDtype...  110 us
    add x1, other arithmetic, on_device(): decay[None, :, None, None] * state_in  2.41 us

profile of v2, /device:TPU:513, one launch (start us, length us, event | category | flops | bytes accessed | tf_op | source)
XLA Modules:
  0.0 114.6 jit_solution(11339782530724137759)
XLA Ops:
  1.3 109.5 %layer_step.1 = (bf16[32,128]{1,0:T(8,128)(2,1)}, f32[8,128]{1,0:T(8,128)}, f32[8,256]{1,0:T(8,128)}) custom-call(bf16[32,128]{1,0:T(8,128)(2,1)} %bitcast.16, bf16[1,32]{1,0:T(2,128)(2,1)} %bitcast.18, bf16[1,32]{1,0:T(2,128)(2,1)} %bitcast.19, bf16[1,32]{1,0:T(2,128)(2,1)} %bitcast.20, f32[1]{0:T(128)S(6)} %copy.21.forget, s32[8]{0:T(128)} %positions.1, ...), custom_call_target="tpu_custom_call" | custom-call | tf_op jit(solution)/shard_map/layer_step/pallas_call | solution.py:346
  110.9 0.0 copy-start.1
  110.9 0.7 copy-done.1
  111.5 0.0 copy-start
  111.5 2.4 %multiply_add_fusion = f32[8,1,128,256]{3,2,1,0:T(8,128)} fusion(f32[8,1,128,256]{3,2,1,0:T(8,128)} %param.30, f32[8,256]{1,0:T(8,128)} %get-tuple-element.7, f32[8,128]{1,0:T(8,128)S(1)} %copy-done.1, f32[]{:T(128)} %bitcast.10), kind=kLoop, calls=%fused_computation | loop fusion | flops 786432 | bytes 2109444 | tf_op jit(solution)/shard_map/add | solution.py:360
  114.0 0.0 copy-done
  114.0 0.6 copy.22
Async XLA Ops:
  110.9 0.7 copy-start.1
  111.5 2.4 %copy-start = (bf16[32,128]{1,0:T(8,128)(2,1)S(1)}, bf16[32,128]{1,0:T(8,128)(2,1)}, u32[]{:S(2)}) copy-start(bf16[32,128]{1,0:T(8,128)(2,1)} %get-tuple-element.5) | copy-start | bytes 24580

commit v3 on v2

v3 whole, which is shorter than its diff:
```python
import functools
import math

import jax
import jax.numpy as jnp
from jax import lax
from jax.experimental import pallas as pl
from jax.experimental.pallas import tpu as pltpu
from jax.sharding import PartitionSpec as P

EPS = 1e-06
BASE = 10000.0
MESH = pl.DeviceIdType.MESH
F32 = jnp.float32
BF16 = jnp.bfloat16


def far_first(n):
    return sorted(range(1, n), key=lambda j: -min(j, n - j))


def near_first(n):
    return sorted(range(1, n), key=lambda j: min(j, n - j))


def widths(total, cut):
    edges = [0, *[c for c in cut if c < total], total]
    return list(zip(edges[:-1], edges[1:]))


def tiles(first, last, step=256):
    return [(at, min(at + step, last)) for at in range(first, last, step)]


def kernel(dims, tokens, gain_in, gain_mix, gain_out, forget, positions,
           gate_in, up_in, down_in, w_query, w_key, w_value, w_gate, w_mix, state,
           gate_out, up_out, down_out,
           result, state_out, *scratch):
    NT, NY, NK, R, OWN, C, c, FF, FP, DK, DV, D, mlp_pieces, qkv_pieces = dims
    (tok_v, gains_v, gi_v, ui_v, di_v, wq_v, wk_v, wv_v, wg_v, wm_v, st_v, go_v, uo_v, do_v, rate_v, place_v, next_v, load_sem,
     xall, ss_src, ssx, ss_k, ss_b, ss_c, ssy, fac,
     part_m, sib_m, red_m, recv_m, part_q, sib_q, red_q, recv_q,
     hall, mall, rows_v, px, rx,
     ax_s, axs_s, sib_s, ssb_s, y_s, ssy_s, ag_s, agf_s, rx_s,
     ax_r, axs_r, sib_r, ssb_r, y_r, ssy_r, ag_r, agf_r, rx_r) = scratch

    t = lax.axis_index("tp")
    k = lax.axis_index("kv")
    core = lax.rem(k, 2)
    y = lax.div(k, 2)
    sibling = {"kv": k + 1 - 2 * core}
    HALF = NY // 2

    def at_t(j):
        return lax.rem(t + j, NT)

    def at_y(j):
        return lax.rem(y + j, NY)

    def chip(j):
        return {"kv": 2 * at_y(j) + core}

    barrier = pltpu.get_barrier_semaphore()
    for j in far_first(NT):
        pl.semaphore_signal(barrier, inc=1, device_id={"tp": at_t(j)}, device_id_type=MESH)
    for j in far_first(NY):
        pl.semaphore_signal(barrier, inc=1, device_id=chip(j), device_id_type=MESH)
    pl.semaphore_signal(barrier, inc=1, device_id=sibling, device_id_type=MESH)

    loads = []
    pairs = [(tokens, tok_v), (gain_in, gains_v.at[0]), (gain_mix, gains_v.at[1]), (gain_out, gains_v.at[2]),
             (gate_in, gi_v), (up_in, ui_v), (w_query, wq_v), (w_key, wk_v), (w_value, wv_v), (w_gate, wg_v),
             (down_in, di_v), (w_mix, wm_v), (state, st_v), (gate_out, go_v), (up_out, uo_v), (down_out, do_v),
             (forget, rate_v), (positions, place_v)]
    for i, (src, dst) in enumerate(pairs):
        if src.shape[0] < dst.shape[0]:
            dst = dst.at[pl.ds(0, src.shape[0])]
        copy = pltpu.make_async_copy(src, dst, load_sem.at[i])
        copy.start()
        loads.append(copy)
    if FP > FF:
        for full in (gi_v, ui_v, di_v, go_v, uo_v, do_v):
            full[FF:] = jnp.zeros((FP - FF, C), BF16)
    for i in range(4):
        loads[i].wait()

    def column(i):
        row = jnp.broadcast_to(gains_v[i].astype(F32), (R, c))
        return row.T

    resid = tok_v[...].astype(F32)
    pl.semaphore_wait(barrier, 1 + (NT - 1) + (NY - 1))

    pending = {}

    def remote(src, dst, ssem, rsem, device):
        return pltpu.make_async_remote_copy(src_ref=src, dst_ref=dst, send_sem=ssem, recv_sem=rsem,
                                            device_id=device, device_id_type=MESH)

    def send(kind, copy):
        copy.start()
        pending.setdefault(kind, []).append(copy)

    def flush(kind):
        for copy in pending.pop(kind, []):
            copy.wait_send()

    @jax.named_scope("gather_x")
    def gather_x(s, normed, squares):
        flush("ax")
        xall[s, t] = normed
        ss_src[s] = squares
        for j in far_first(NT):
            send("ax", remote(xall.at[s, t], xall.at[s, t], ax_s.at[j], ax_r.at[s, NT - j], {"tp": at_t(j)}))
        for j in far_first(NT):
            send("ax", remote(ss_src.at[s], ssx.at[s, NT - j], axs_s.at[j], axs_r.at[s, NT - j], {"tp": at_t(j)}))
        for j in near_first(NT):
            remote(xall.at[s, t], xall.at[s, t], ax_s.at[j], ax_r.at[s, j], {"tp": at_t(j)}).wait_recv()
        whole = xall[s].astype(F32).reshape(C, R)
        return whole.T.astype(BF16)

    class Reduce:
        def __init__(self, s, part, sib, red, recv, relay, squares):
            self.s, self.part, self.sib, self.red, self.recv = s, part, sib, red, recv
            self.relay, self.squares = relay, squares
            flush("y")

        def side(self, p):
            return 1 if p % 2 == 0 else NY - 1

        def swap(self, p):
            return remote(self.part[p].at[1 - core], self.sib[p], sib_s.at[p], sib_r.at[self.s, p], sibling)

        def hop(self, p, j, device_j, slot):
            return remote(self.red[p].at[at_y(j)], self.recv[p].at[slot], y_s.at[p, j], y_r.at[self.s, p, slot],
                          chip(device_j))

        def arrived(self, p, slot):
            self.hop(p, slot, slot, slot).wait_recv()
            return self.recv[p][slot].astype(F32)

        def both(self, p, yd):
            return self.part[p][core, yd].astype(F32) + self.sib[p][yd].astype(F32)

        def start_squares(self):
            s, block = self.s, self.squares
            for j in near_first(NT):
                remote(ss_src.at[s], ssx.at[s, j], axs_s.at[j], axs_r.at[s, j], {"tp": at_t(j)}).wait_recv()
                block = block + ssx[s, j]
            ss_k[s] = block
            self.block = block
            send("y", remote(ss_k.at[s], ss_b.at[s], ssb_s.at[0], ssb_r.at[s], sibling))

        def send_squares(self):
            s = self.s
            remote(ss_k.at[s], ss_b.at[s], ssb_s.at[0], ssb_r.at[s], sibling).wait_recv()
            self.block = self.block + ss_b[s]
            ss_c[s] = self.block
            for j in far_first(NY):
                send("y", remote(ss_c.at[s], ssy.at[s, NY - j], ssy_s.at[j], ssy_r.at[s, NY - j], chip(j)))

        def factor(self):
            s, total = self.s, self.block
            for j in near_first(NY):
                remote(ss_c.at[s], ssy.at[s, j], ssy_s.at[j], ssy_r.at[s, j], chip(j)).wait_recv()
                total = total + ssy[s, j]
            fac[s] = lax.rsqrt(jnp.broadcast_to(total, (128, R)).T / D + EPS)
            return fac[s, pl.ds(pl.multiple_of(k * OWN, OWN), OWN), :][:, :1]

        @jax.named_scope("send_piece")
        def send_piece(self, p):
            self.swap(p).wait_recv()
            side = self.side(p)
            late = None
            for j in far_first(NY):
                last = HALF - 1 if side == 1 else HALF + 1
                if self.relay and j == last:
                    continue
                yd = at_y(j)
                self.red[p][yd] = self.both(p, yd).astype(BF16)
                if late is not None:
                    send("y", late)
                if self.relay and j == HALF:
                    late = self.hop(p, j, side, HALF)
                else:
                    late = self.hop(p, j, j, NY - j)
            send("y", late)

        @jax.named_scope("send_relayed")
        def send_relayed(self, p):
            if not self.relay:
                return
            last = HALF - 1 if self.side(p) == 1 else HALF + 1
            yd = at_y(last)
            self.red[p][yd] = (self.both(p, yd) + self.arrived(p, HALF)).astype(BF16)
            send("y", self.hop(p, last, last, NY - last))

        @jax.named_scope("collect")
        def collect(self, p):
            acc = self.both(p, y)
            for j in near_first(NY):
                if not (self.relay and j == HALF):
                    acc = acc + self.arrived(p, j)
            return acc

    class Gather:
        def __init__(self, s, bufs, relay):
            self.s, self.bufs, self.relay = s, bufs, relay
            flush("ag")

        def same(self, p, slot, j, device_j, off):
            ref = self.bufs[p].at[slot]
            return remote(ref, ref, ag_s.at[p, j], ag_r.at[self.s, p, off], chip(device_j))

        def over(self, p, slot, off):
            ref = self.bufs[p].at[slot]
            return remote(ref, ref, agf_s.at[p, off], agf_r.at[self.s, p, off], sibling)

        def start(self, p):
            for j in far_first(NY):
                if not (self.relay and j == HALF):
                    send("ag", self.same(p, k, j, j, NY - j))
            send("ag", self.over(p, k, 0))

        @jax.named_scope("forward")
        def forward(self, p):
            side = 1 if p % 2 == 0 else NY - 1
            source = HALF + 1 if side == 1 else HALF - 1
            order = [j for j in near_first(NY) if j != HALF]
            order.sort(key=lambda j: (min(j, NY - j), j != source))
            for j in order + [HALF]:
                slot = 2 * at_y(j) + core
                self.same(p, slot, j, j, j).wait_recv()
                if self.relay and j == source:
                    send("ag", self.same(p, slot, HALF, side, HALF))
                send("ag", self.over(p, slot, j))

        @jax.named_scope("finish")
        def finish(self, p, rows, first, last):
            for j in [0] + near_first(NY):
                yd = at_y(j)
                self.over(p, 2 * yd + 1 - core, j).wait_recv()
                pair = jnp.concatenate([self.bufs[p][2 * yd].astype(F32), self.bufs[p][2 * yd + 1].astype(F32)], axis=0)
                rows[pl.ds(pl.multiple_of(2 * OWN * yd, 2 * OWN), 2 * OWN), first:last] = pair.astype(BF16)

    @jax.named_scope("scatter_x")
    def scatter_x(s, product):
        flush("rx")
        px[s] = product.T.reshape(NT, c, R).astype(BF16)
        for j in far_first(NT):
            send("rx", remote(px.at[s, at_t(j)], rx.at[s, NT - j], rx_s.at[j], rx_r.at[s, NT - j], {"tp": at_t(j)}))
        total = px[s, t].astype(F32)
        for j in near_first(NT):
            remote(px.at[s, at_t(j)], rx.at[s, j], rx_s.at[j], rx_r.at[s, j], {"tp": at_t(j)}).wait_recv()
            total = total + rx[s, j].astype(F32)
        return total

    def half_mlp(s, resid, gain, gate, up, down, waits):
        m = s // 2
        count = len(mlp_pieces)
        squares = jnp.sum(resid * resid, axis=0, keepdims=True)
        normed = gather_x(s, (resid * gain).astype(BF16), squares)
        for i in waits[:2]:
            loads[i].wait()
        reduce = Reduce(s, part_m, sib_m, red_m, [r.at[m] for r in recv_m], False, squares)
        for p, (first, last) in enumerate(mlp_pieces):
            with jax.named_scope("mm_up"):
                for lo, hi in tiles(first, last):
                    g = lax.dot_general(normed, gate[lo:hi], (((1,), (1,)), ((), ())), preferred_element_type=F32)
                    u = lax.dot_general(normed, up[lo:hi], (((1,), (1,)), ((), ())), preferred_element_type=F32)
                    for kk in range(NK):
                        rows = slice(OWN * kk, OWN * kk + OWN)
                        part_m[p][kk % 2, kk // 2, :, lo - first:hi - first] = jnp.concatenate(
                            [g[rows], u[rows]], axis=0).astype(BF16)
            send("y", reduce.swap(p))
            if p == 0:
                reduce.start_squares()
        reduce.send_squares()
        for p in range(count):
            reduce.send_piece(p)
            if p:
                reduce.send_relayed(p - 1)
        reduce.send_relayed(count - 1)
        factor = reduce.factor()
        gather = Gather(s, [h.at[m] for h in hall], False)
        for p in range(count):
            acc = reduce.collect(p)
            g = factor * acc[:OWN]
            u = factor * acc[OWN:]
            hall[p][m, k] = (g / (1.0 + jnp.exp(-g)) * u).astype(BF16)
            gather.start(p)
        loads[waits[2]].wait()
        product = None
        for p in range(count + 1):
            if p < count:
                gather.forward(p)
            if p:
                first, last = mlp_pieces[p - 1]
                gather.finish(p - 1, rows_v, first, last)
                term = jnp.dot(rows_v[:, first:last], down[first:last], preferred_element_type=F32)
                product = term if product is None else product + term
        return resid + 0.5 * scatter_x(s, product)

    resid = half_mlp(0, resid, column(0), gi_v, ui_v, di_v, (4, 5, 10)).astype(BF16).astype(F32)

    squares = jnp.sum(resid * resid, axis=0, keepdims=True)
    normed = gather_x(1, (resid * column(1)).astype(BF16), squares)
    for i in (6, 7, 8, 9, 16, 17):
        loads[i].wait()
    reduce = Reduce(1, part_q, sib_q, red_q, recv_q, False, squares)
    q = jnp.dot(normed, wq_v[...], preferred_element_type=F32)
    key = jnp.dot(normed, wk_v[...], preferred_element_type=F32)
    value = jnp.dot(normed, wv_v[...], preferred_element_type=F32)
    out_gate = jnp.dot(normed, wg_v[...], preferred_element_type=F32)
    half = DV // 2
    top = [q, key, value[:, :half]]
    low = [value[:, half:], out_gate[:, :half], out_gate[:, half:]]
    for i in range(3):
        for kk in range(NK):
            rows = slice(OWN * kk, OWN * kk + OWN)
            part_q[0][kk % 2, kk // 2, :, DK * i:DK * i + DK] = jnp.concatenate(
                [top[i][rows], low[i][rows]], axis=0).astype(BF16)
    send("y", reduce.swap(0))
    reduce.start_squares()
    reduce.send_squares()
    reduce.send_piece(0)

    row = lax.broadcasted_iota(jnp.int32, (OWN, DK), 0)
    lane = lax.broadcasted_iota(jnp.int32, (OWN, DK), 1)
    place = jnp.zeros((OWN, DK), F32)
    for r in range(OWN):
        place = jnp.where(row == r, place_v[r].astype(F32), place)
    half = DK // 2
    pair = jnp.where(lane < half, lane, lane - half).astype(F32)
    angle = place * jnp.exp(pair * (-2.0 * math.log(BASE) / DK))
    cosine = jnp.cos(angle)
    sine = jnp.where(lane < half, -jnp.sin(angle), jnp.sin(angle))
    decay = jnp.exp(-jnp.broadcast_to(rate_v[...], (1, DV)))
    loads[12].wait()

    factor = reduce.factor()
    acc = reduce.collect(0)
    acc = (jnp.concatenate([factor, factor], axis=0) * acc).astype(BF16).astype(F32)
    q, key = acc[:OWN, :DK], acc[:OWN, DK:2 * DK]
    value = jnp.concatenate([acc[:OWN, 2 * DK:], acc[OWN:, :DK]], axis=1)
    out_gate = acc[OWN:, DK:]

    def rotate(v):
        return v * cosine + jnp.concatenate([v[:, half:], v[:, :half]], axis=1) * sine

    with jax.named_scope("retain"):
        q = rotate(q)
        key = rotate(key) * DK ** (-0.5)
        q_col = q.T
        carried = jnp.concatenate(
            [jnp.sum(st_v[b] * q_col[:, b:b + 1], axis=0, keepdims=True) for b in range(OWN)], axis=0)
        retained = jnp.sum(q * key, axis=1, keepdims=True) * value + decay * carried
        scaled = retained * lax.rsqrt(jnp.mean(retained * retained, axis=1, keepdims=True) + EPS)
        gather = Gather(1, [mall], False)
        mall[k] = (out_gate / (1.0 + jnp.exp(-out_gate)) * scaled).astype(BF16)
        gather.start(0)
    with jax.named_scope("new_state"):
        key_col = key.T
        for b in range(OWN):
            next_v[b] = decay * st_v[b] + key_col[:, b:b + 1] * value[b:b + 1, :]
        keep = pltpu.make_async_copy(next_v, state_out, load_sem.at[18])
        keep.start()
    loads[11].wait()
    gather.forward(0)
    gather.finish(0, rows_v, 0, DV)
    product = jnp.dot(rows_v[:, :DV], wm_v[...], preferred_element_type=F32)
    resid = (resid + scatter_x(1, product)).astype(BF16).astype(F32)

    out = half_mlp(2, resid, column(2), go_v, uo_v, do_v, (13, 14, 15))
    result[...] = out.astype(BF16)
    keep.wait()
    for kind in ("ax", "y", "ag", "rx"):
        flush(kind)


def on_device(tokens, gain_in, gate_in, up_in, down_in, gain_mix, w_query, w_key, w_value, w_gate,
              w_mixout, forget_rate, state_in, positions, gain_out, gate_out, up_out, down_out):
    NT = lax.axis_size("tp")
    NK = lax.axis_size("kv")
    NY = NK // 2
    R, c = tokens.shape
    C, FF = gate_in.shape
    OWN, _, DK, DV = state_in.shape
    D = C * NK
    FP = -(-FF // 128) * 128
    mlp_pieces = widths(FP, (768,))
    qkv_pieces = [(0, 3 * DK)]
    dims = (NT, NY, NK, R, OWN, C, c, FF, FP, DK, DV, D, mlp_pieces, qkv_pieces)

    def exchange(pieces, calls):
        wide = [last - first for first, last in pieces]
        return (
            [pltpu.VMEM((2, NY, 2 * OWN, w), BF16) for w in wide],
            [pltpu.VMEM((NY, 2 * OWN, w), BF16) for w in wide],
            [pltpu.VMEM((NY, 2 * OWN, w), BF16) for w in wide],
            [pltpu.VMEM((*calls, NY, 2 * OWN, w), BF16) for w in wide],
        )

    dma = pltpu.SemaphoreType.DMA
    n_p = len(mlp_pieces)
    scratch = [
        pltpu.VMEM((c, R), BF16), pltpu.VMEM((3, 1, c), BF16),
        pltpu.VMEM((FP, C), BF16), pltpu.VMEM((FP, C), BF16), pltpu.VMEM((FP, C), BF16),
        pltpu.VMEM((C, DK), BF16), pltpu.VMEM((C, DK), BF16), pltpu.VMEM((C, DV), BF16), pltpu.VMEM((C, DV), BF16),
        pltpu.VMEM((DV, C), BF16), pltpu.VMEM((OWN, DK, DV), F32),
        pltpu.VMEM((FP, C), BF16), pltpu.VMEM((FP, C), BF16), pltpu.VMEM((FP, C), BF16),
        pltpu.VMEM((1, 1), F32), pltpu.SMEM((OWN,), jnp.int32), pltpu.VMEM((OWN, DK, DV), F32), dma((19,)),
        pltpu.VMEM((3, NT, c, R), BF16), pltpu.VMEM((3, 1, R), F32), pltpu.VMEM((3, NT, 1, R), F32),
        pltpu.VMEM((3, 1, R), F32), pltpu.VMEM((3, 1, R), F32), pltpu.VMEM((3, 1, R), F32),
        pltpu.VMEM((3, NY, 1, R), F32), pltpu.VMEM((3, R, 128), F32),
        *exchange(mlp_pieces, (2,)),
        *exchange(qkv_pieces, ()),
        [pltpu.VMEM((2, NK, OWN, b - a), BF16) for a, b in mlp_pieces], pltpu.VMEM((NK, OWN, DV), BF16),
        pltpu.VMEM((R, FP), BF16),
        pltpu.VMEM((3, NT, c, R), BF16), pltpu.VMEM((3, NT, c, R), BF16),
        dma((NT,)), dma((NT,)), dma((n_p,)), dma((1,)), dma((n_p, NY)), dma((NY,)), dma((n_p, NY)), dma((n_p, NY)),
        dma((NT,)),
        dma((3, NT)), dma((3, NT)), dma((3, n_p)), dma((3,)), dma((3, n_p, NY)), dma((3, NY)), dma((3, n_p, NY)),
        dma((3, n_p, NY)), dma((3, NT)),
    ]
    hbm = pl.BlockSpec(memory_space=pltpu.HBM)
    vmem = pl.BlockSpec(memory_space=pltpu.VMEM)
    result, new_state = pl.pallas_call(
        functools.partial(kernel, dims),
        out_shape=(jax.ShapeDtypeStruct((c, R), BF16), jax.ShapeDtypeStruct((OWN, DK, DV), F32)),
        in_specs=[hbm] * 18,
        out_specs=(vmem, hbm),
        scratch_shapes=scratch,
        compiler_params=pltpu.CompilerParams(collective_id=0, has_side_effects=True,
                                             vmem_limit_bytes=67043328),
        name="layer_step",
    )(tokens.T, gain_in[None], gain_mix[None], gain_out[None], forget_rate[None], positions,
      gate_in.T, up_in.T, down_in, w_query, w_key, w_value, w_gate, w_mixout, state_in.reshape(OWN, DK, DV),
      gate_out.T, up_out.T, down_out)
    return result.T, new_state.reshape(state_in.shape)


KV_TP = ("kv", "tp")


def solution(mesh):
    feature, wide, tall = P(KV_TP), P("kv", "tp"), P("tp", "kv")
    state = P(("grp", "kv"), "tp", None, None)
    placed = (P("grp", KV_TP), feature, wide, wide, tall, feature, wide, wide, wide, wide, tall, P("tp"), state,
              P(("grp", "kv")), feature, wide, wide, tall)
    return jax.shard_map(on_device, mesh=mesh, in_specs=placed, out_specs=(P("grp", KV_TP), state), check_vma=False)
```

time: 115 us -> 108 us (0.939)
  Pallas kernels: 110 us -> 103 us
  other arithmetic: 2.41 us -> 0 us
  local copies, waits for them, and re-layouts: 1.27 us -> 3.56 us
    pallas_call x1, Pallas kernels: 110 us -> 103 us  [on_device(): pl.pallas_call(functools.partial(kernel, dims), out_shape=(jax.ShapeDtype...]
    add x1 -> x0, other arithmetic: 2.41 us -> none  [on_device(): decay[None, :, None, None] * state_in]
    unnamed x5 -> x2, local copies, waits for them, and re-layouts: 1.27 us -> 3.56 us
where the time goes in v3:
time: 108 us
  Pallas kernels  103 us (95%)
  local copies, waits for them, and re-layouts  3.56 us (3%)
  between operations  1.29 us (1%)
    pallas_call x1, Pallas kernels, on_device(): pl.pallas_call(functools.partial(kernel, dims), out_shape=(jax.ShapeDtype...  103 us
    unnamed x2, local copies, waits for them, and re-layouts  3.56 us

profile of v3, /device:TPU:513, one launch (start us, length us, event | category | flops | bytes accessed | tf_op | source)
XLA Modules:
  0.0 108.3 jit_solution(11357532182727269790)
XLA Ops:
  1.3 103.4 %layer_step.1 = (bf16[32,128]{1,0:T(8,128)(2,1)}, f32[8,128,256]{2,1,0:T(8,128)}) custom-call(bf16[32,128]{1,0:T(8,128)(2,1)} %bitcast.21, bf16[1,32]{1,0:T(2,128)(2,1)} %bitcast.23, bf16[1,32]{1,0:T(2,128)(2,1)} %bitcast.24, bf16[1,32]{1,0:T(2,128)(2,1)} %bitcast.25, f32[1,1]{1,0:T(1,128)} %bitcast.14.forget, s32[8]{0:T(128)} %positions.1, ...), custom_call_target="tpu_custom_call" | custom-call | tf_op jit(solution)/shard_map/layer_step/pallas_call | solution.py:428
  104.7 1.3 %copy.24 = bf16[128,32]{0,1:T(8,128)(2,1)} copy(bf16[128,32]{0,1:T(8,128)(2,1)} %bitcast.22) | data formatting | bytes 16384
  106.0 2.3 %copy.25 = f32[8,1,128,256]{3,2,1,0:T(8,128)} copy(f32[8,1,128,256]{3,2,1,0:T(8,128)} %bitcast.15) | data formatting | bytes 2097152
